TPU v7x, 256 devices: a whole 4x4x8 slice. The times are simulated.
256 devices in a mesh: ep: 64 (over z, y, core), tp: 4 (over x).
Axes of the slice: x: 4, y: 4, z: 8, core: 2. Of those that a mesh axis runs over, the one named last changes fastest.
Arguments:
- mixer_in: bfloat16 [32768, 4096], P(('ep', 'tp')), may hold values from -6 to 6
- mixer_gain: float32 [4096], replicated, may hold values from 0.1 to 1.9
- group_weight: bfloat16 [4, 1024, 1024], P('tp'), may hold values from -0.1875 to 0.1875
- group_scale: float32 [4, 1024], P('tp'), may hold values from 0.1 to 1.9
- expert_in: bfloat16 [32768, 4096], P(('ep', 'tp')), may hold values from -6 to 6
- expert_gain: float32 [4096], replicated, may hold values from 0.1 to 1.9
- routes: int32 [32768, 2], P('ep'), may hold values from 0 to 63, all different within a row; in each aligned block of 128 rows (0 to 127, 128 to 255, ...) at most 6 rows name the same one
- route_weight: float32 [32768, 2], P('ep'), may hold values from 0.2 to 1
- gate_weight: bfloat16 [64, 4096, 1024], P('ep', None, 'tp'), may hold values from -0.25 to 0.25
- up_weight: bfloat16 [64, 4096, 1024], P('ep', None, 'tp'), may hold values from -0.25 to 0.25
- down_weight: bfloat16 [64, 1024, 4096], P('ep', 'tp'), may hold values from -0.02734375 to 0.02734375
Outputs:
- mixed: bfloat16 [32768, 4096], P('ep', 'tp')
- expert_out: bfloat16 [32768, 4096], P(('ep', 'tp'))
Inputs may be any that keep to these rules, and one draw needn't show every extreme that they name: `routes`: each row names 2 different experts; within the rows of one device (aligned blocks of 128 rows) no expert is named more than 6 times, and that count is reached.
All inputs are finite; a program needn't handle non-finite values.
Results may differ from a plain program's by a relative error of at most 0.012.
Values may be sent and summed in bfloat16 or wider, within the bound.
A program may use at most 128 MiB of HBM per device.

v0:
```python
import jax
import jax.numpy as jnp
from jax import lax
from jax.sharding import PartitionSpec as P

WMAX = 16
TOP = 2
epsilon = 1e-06
clamp_limit = 7.0
sigmoid_slope = 1.702


def from_behind(x, axis, by):
    count = lax.axis_size(axis)
    pairs = [(i, i + by) for i in range(count) if 0 <= i + by < count]
    return lax.ppermute(x, axis, pairs)


def rms_norm(values, gain):
    widened = values.astype(jnp.float32)
    scaled = widened * lax.rsqrt(jnp.mean(widened * widened, axis=-1, keepdims=True) + epsilon)
    return (scaled * gain).astype(jnp.bfloat16)


def clamped_unit(gate_part, up_part):
    gate_part = jnp.minimum(gate_part, clamp_limit)
    up_part = jnp.clip(up_part, -clamp_limit, clamp_limit)
    return ((up_part + 1.0) * gate_part * jax.nn.sigmoid(sigmoid_slope * gate_part)).astype(
        jnp.bfloat16
    )


def slot_table(block_routes, experts, capacity):
    count = block_routes.shape[0]
    onehot = (
        block_routes[:, :, None] == jnp.arange(experts, dtype=jnp.int32)[None, None, :]
    ).astype(jnp.int32)
    per_token = jnp.sum(onehot, axis=1)
    earlier = jnp.cumsum(per_token, axis=0) - per_token
    slot_rank = jnp.sum(onehot * earlier[:, None, :], axis=2)
    matches = onehot[:, :, :, None] * (
        slot_rank[:, :, None, None] == jnp.arange(capacity, dtype=jnp.int32)[None, None, None, :]
    ).astype(jnp.int32)
    source = jnp.sum(matches * jnp.arange(count, dtype=jnp.int32)[:, None, None, None], axis=(0, 1))
    filled = jnp.sum(matches, axis=(0, 1))
    return (source, filled, slot_rank)


def shards(
    mixer_in,
    mixer_gain,
    group_weight,
    group_scale,
    expert_in,
    expert_gain,
    routes,
    route_weight,
    gate_weight,
    up_weight,
    down_weight,
):
    normed = rms_norm(mixer_in, mixer_gain)
    shard_rows = lax.all_to_all(normed, "tp", split_axis=1, concat_axis=0, tiled=True)
    length = shard_rows.shape[0]
    last_rows = shard_rows[length - (WMAX - 1) :]
    before = from_behind(last_rows, "ep", 1)
    extended = jnp.concatenate([before, shard_rows], axis=0).astype(jnp.float32)
    window = 2 << lax.axis_index("tp")
    position = lax.axis_index("ep") * length + jnp.arange(length, dtype=jnp.int32)
    prefix = jnp.concatenate(
        [jnp.zeros((1, extended.shape[1]), jnp.float32), jnp.cumsum(extended, axis=0)], axis=0
    )
    upper = prefix[WMAX:]
    lower = lax.dynamic_slice_in_dim(prefix, WMAX - window, length, 0)
    counts = jnp.minimum(position + 1, window).astype(jnp.float32)[:, None]
    pooled = ((upper - lower) / counts - extended[WMAX - 1 :]).astype(jnp.bfloat16)
    mixed = (
        jnp.dot(pooled, group_weight[0], preferred_element_type=jnp.float32) * group_scale[0]
    ).astype(jnp.bfloat16)
    expert_norm = rms_norm(expert_in, expert_gain)
    tok_count = expert_in.shape[0]
    width = expert_in.shape[1]
    experts = lax.axis_size("ep")
    capacity = max(2, 3 * tok_count * TOP // (2 * experts))
    tp_index = lax.axis_index("tp")
    own_routes = lax.dynamic_slice_in_dim(routes, tp_index * tok_count, tok_count, 0)
    own_weight = lax.dynamic_slice_in_dim(route_weight, tp_index * tok_count, tok_count, 0)
    gate_local = gate_weight[0]
    up_local = up_weight[0]
    source, filled, own_rank = slot_table(own_routes, experts, capacity)
    outgoing = expert_norm[source] * filled[:, :, None].astype(jnp.bfloat16)
    arrived = lax.all_to_all(outgoing, "ep", split_axis=0, concat_axis=0, tiled=True)
    piece = lax.all_gather(arrived.reshape(-1, width), "tp", axis=0, tiled=True)
    hidden = clamped_unit(
        jnp.dot(piece, gate_local, preferred_element_type=jnp.float32),
        jnp.dot(piece, up_local, preferred_element_type=jnp.float32),
    )
    down_local = down_weight[0]
    part_width = down_local.shape[0]
    unit_block = lax.all_to_all(hidden, "tp", split_axis=0, concat_axis=1, tiled=True)
    empty = jnp.zeros((unit_block.shape[0], width), jnp.float32)
    total = empty
    piece = lax.all_gather(down_local, "tp", axis=0, tiled=True)
    for part in range(piece.shape[0] // part_width):
        columns = lax.dynamic_slice_in_dim(unit_block, part * part_width, part_width, 1)
        partial_value = jnp.dot(
            columns,
            piece[part * part_width : (part + 1) * part_width],
            preferred_element_type=jnp.float32,
        ).astype(jnp.bfloat16)
        total = total + lax.optimization_barrier(partial_value).astype(jnp.float32)
    summed = total
    summed = summed.astype(jnp.bfloat16).reshape(experts, capacity, width)
    returned = lax.all_to_all(summed, "ep", split_axis=0, concat_axis=0, tiled=True)
    flat_rows = returned.reshape(-1, width)
    slot_index = own_routes * capacity + own_rank
    expert_sum = jnp.zeros((tok_count, width), jnp.float32)
    for choice_slot in range(TOP):
        expert_sum = (
            expert_sum
            + flat_rows[slot_index[:, choice_slot]].astype(jnp.float32)
            * own_weight[:, choice_slot : choice_slot + 1]
        )
    return (mixed, expert_sum.astype(jnp.bfloat16))


def solution(mesh):
    in_specs = (
        P(("ep", "tp"), None),
        P(),
        P("tp", None, None),
        P("tp", None),
        P(("ep", "tp"), None),
        P(),
        P("ep", None),
        P("ep", None),
        P("ep", None, "tp"),
        P("ep", None, "tp"),
        P("ep", "tp", None),
    )
    out_specs = (P("ep", "tp"), P(("ep", "tp"), None))
    return jax.shard_map(shards, mesh=mesh, in_specs=in_specs, out_specs=out_specs, check_vma=False)
```

profile of v0, /device:TPU:96, one launch (start us, length us, event | category | flops | bytes accessed | tf_op | source)
XLA Modules:
  0.0 527.5 jit_solution(16319428711208255795)
XLA Ops:
  7.2 0.8 constant_dynamic-slice_fusion.1
  8.5 0.3 multiply_reduce_fusion
  9.0 1.5 fusion.12
  10.6 1.6 fusion.14
  12.1 4.1 gather_fusion
  16.2 5.7 %reshape.101 = bf16[64,6,4096]{2,1,0:T(8,128)(2,1)} reshape(bf16[384,4096]{1,0:T(8,128)(2,1)} %gather_fusion) | data formatting | bytes 6291456 | tf_op jit(solution)/shard_map/gather | solution.py:91
  22.0 2.5 broadcast_multiply_fusion
  24.5 105.1 %all_to_all.48 = bf16[64,6,4096]{2,1,0:T(8,128)(2,1)} all-to-all(bf16[64,6,4096]{2,1,0:T(8,128)(2,1)S(1)} %broadcast_multiply_fusion), channel_id=1, replica_groups=mesh['ep'=64,'tp'=4] {'ep'}, dimensions={0} | all-to-all | bytes 6291456 | tf_op jit(solution)/shard_map/all_to_all | solution.py:92
  129.7 5.7 %reshape.97 = bf16[384,4096]{1,0:T(8,128)(2,1)} reshape(bf16[64,6,4096]{2,1,0:T(8,128)(2,1)} %all_to_all.48) | data formatting | bytes 6291456 | tf_op jit(solution)/shard_map/reshape | solution.py:93
  135.5 0.7 all-gather.6.cloned.1.call-update
  136.2 1.6 copy.27
  137.8 0.6 fusion.9
  138.4 116.5 %all-gather.4.cloned.1.call-done = bf16[1536,4096]{1,0:T(8,128)(2,1)} async-done(((bf16[384,4096]{1,0:T(8,128)(2,1)}), bf16[1536,4096]{1,0:T(8,128)(2,1)}) %all-gather.4.cloned.1.call-update) | async-done | bytes 12582928 | tf_op jit(solution)/shard_map/all_gather | solution.py:93
  254.9 7.7 %convolution_minimum_fusion = f32[1536,256]{1,0:T(8,128)S(1)} fusion(bf16[1536,4096]{1,0:T(8,128)(2,1)} %all-gather.4.cloned.1.call-done, bf16[1,4096,256]{2,1,0:T(8,128)(2,1)} %param.19), kind=kOutput, calls=%fused_computation.10 | convolution fusion | flops 3221618688 | bytes 16252928 | tf_op jit(solution)/shard_map/dot_general | solution.py:95
  262.6 1.0 copy-done.6
  263.7 0.6 copy-done.7
  264.3 4.9 fusion.5
  269.2 2.4 copy.36
  271.6 4.2 all-to-all-start.2
  275.8 1.5 fusion.11
  277.3 20.3 %all-to-all-done.2 = bf16[4,384,256]{1,2,0:T(8,128)(2,1)} async-done(((bf16[4,384,256]{1,2,0:T(8,128)(2,1)}), bf16[4,384,256]{1,2,0:T(8,128)(2,1)}, u32[]{:S(2)}, u32[]{:S(2)}) %all-to-all-start.2) | async-done | bytes 786464 | tf_op jit(solution)/shard_map/all_to_all | solution.py:100
  297.6 3.7 all-to-all-start
  301.3 61.7 %all-gather.6.cloned.1.call-done = bf16[1,1024,4096]{2,1,0:T(8,128)(2,1)} async-done(((bf16[1,256,4096]{2,1,0:T(8,128)(2,1)}), bf16[1,1024,4096]{2,1,0:T(8,128)(2,1)}) %all-gather.6.cloned.1.call-update) | async-done | bytes 8388624 | tf_op jit(solution)/shard_map/all_gather | solution.py:103
  363.0 2.8 convolution_convert_fusion.3
  365.8 3.0 convolution_convert_fusion.2
  368.8 1.9 convolution_convert_fusion.1
  370.8 1.9 convolution_convert_fusion
  372.7 4.1 add_convert_fusion
  376.8 5.7 %reshape.98 = bf16[64,6,4096]{2,1,0:T(8,128)(2,1)} reshape(bf16[384,4096]{1,0:T(8,128)(2,1)} %add_convert_fusion) | data formatting | bytes 6291456 | tf_op jit(solution)/shard_map/reshape | solution.py:113
  382.5 1.0 copy-done.3
  383.5 10.5 %all-to-all-start.3 = ((bf16[64,6,4096]{2,1,0:T(8,128)(2,1)}), bf16[64,6,4096]{2,1,0:T(8,128)(2,1)}, u32[]{:S(2)}, u32[]{:S(2)}) async-start(bf16[64,6,4096]{2,1,0:T(8,128)(2,1)} %reshape.98), calls=%async_computation.3 | async-start | bytes 8388608 | tf_op jit(solution)/shard_map/all_to_all | solution.py:114
  394.0 0.7 constant_dynamic-slice_fusion
  394.7 0.7 multiply_add_fusion
  395.4 1.5 copy.28
  396.9 2.3 collective-permute-start
  399.2 88.1 %collective-permute-done = bf16[15,1024]{1,0:T(8,128)(2,1)S(1)} collective-permute-done((bf16[15,1024]{1,0:T(8,128)(2,1)S(1)}, bf16[15,1024]{1,0:T(8,128)(2,1)S(1)}, u32[]{:S(2)}, u32[]{:S(2)}) %collective-permute-start) | collective-permute-done | bytes 30752 | tf_op jit(solution)/shard_map/ppermute | solution.py:16
  487.3 1.7 fusion.29
  489.0 0.3 pad.4
  489.3 2.6 fusion
  491.9 2.0 copy-done.1
  493.9 2.6 broadcast_add_fusion
  496.5 1.5 copy.30
  498.3 1.3 copy-done.4
  499.7 2.6 multiply_convert_fusion
  502.3 5.7 %reshape.99 = bf16[384,4096]{1,0:T(8,128)(2,1)} reshape(bf16[64,6,4096]{2,1,0:T(8,128)(2,1)} %all-to-all-done.3) | data formatting | bytes 6291456 | tf_op jit(solution)/shard_map/reshape | solution.py:115
  508.0 4.5 gather_fusion.1
  512.5 5.5 %gather_fusion.2 = bf16[128,4096]{1,0:T(8,128)(2,1)} fusion(bf16[384,4096]{1,0:T(8,128)(2,1)} %reshape.99, s32[1024]{0:T(1024)S(1)} %get-tuple-element.10), kind=kCustom, calls=%fused_computation.2 | custom fusion | bytes 2097664 | tf_op jit(solution)/shard_map/gather | solution.py:121
  518.0 2.7 add_convert_fusion.1
  (42 shorter events, 1.2 us)
Async XLA Ops:
  7.2 491.2 %copy-start = (bf16[1,1024,1024]{2,1,0:T(8,128)(2,1)S(1)}, bf16[1,1024,1024]{2,1,0:T(8,128)(2,1)}, u32[]{:S(2)}) copy-start(bf16[1,1024,1024]{2,1,0:T(8,128)(2,1)} %param.13) | copy-start | bytes 6291460
  7.2 247.7 %all-gather.4.cloned.1.call-start = ((), (), s32[]{:S(2)}) async-start(), calls=%async_computation.4 | async-start | bytes 15728640 | tf_op jit(solution)/shard_map/all_gather | solution.py:93
  135.4 227.6 %all-gather.6.cloned.1.call-start = ((), (), s32[]{:S(2)}) async-start(), calls=%async_computation.5 | async-start | bytes 10485760 | tf_op jit(solution)/shard_map/all_gather | solution.py:103
  254.9 8.8 %copy-start.6 = (bf16[1536,4096]{1,0:T(8,128)(2,1)S(1)}, bf16[1536,4096]{1,0:T(8,128)(2,1)}, u32[]{:S(2)}) copy-start(bf16[1536,4096]{1,0:T(8,128)(2,1)} %all-gather.4.cloned.1.call-done) | copy-start | bytes 37748740
  254.9 9.4 %copy-start.7 = (bf16[1,4096,256]{2,1,0:T(8,128)(2,1)S(1)}, bf16[1,4096,256]{2,1,0:T(8,128)(2,1)}, u32[]{:S(2)}) copy-start(bf16[1,4096,256]{2,1,0:T(8,128)(2,1)} %param.20) | copy-start | bytes 6291460
  269.2 6.6 %copy-start.5 = (f32[4096]{0:T(1024)S(1)}, f32[4096]{0:T(1024)}, u32[]{:S(2)}) copy-start(f32[4096]{0:T(1024)} %param.12) | copy-start | bytes 49156
  271.6 26.0 %all-to-all-start.2 = ((bf16[4,384,256]{1,2,0:T(8,128)(2,1)}), bf16[4,384,256]{1,2,0:T(8,128)(2,1)}, u32[]{:S(2)}, u32[]{:S(2)}) async-start(bf16[4,384,256]{1,2,0:T(8,128)(2,1)} %copy.36), calls=%async_computation.2 | async-start | bytes 1572864 | tf_op jit(solution)/shard_map/all_to_all | solution.py:100
  297.6 84.9 %all-to-all-start = ((bf16[128,4,1024]{0,2,1:T(8,128)(2,1)}), bf16[128,4,1024]{0,2,1:T(8,128)(2,1)S(1)}, u32[]{:S(2)}, u32[]{:S(2)}) async-start(bf16[128,4,1024]{0,2,1:T(8,128)(2,1)} %bitcast.59), calls=%async_computation | async-start | bytes 2097152 | tf_op jit(solution)/shard_map/all_to_all | solution.py:63
  363.0 5.8 %copy-start.2 = (bf16[1,1024,4096]{2,1,0:T(8,128)(2,1)S(1)}, bf16[1,1024,4096]{2,1,0:T(8,128)(2,1)}, u32[]{:S(2)}) copy-start(bf16[1,1024,4096]{2,1,0:T(8,128)(2,1)} %all-gather.6.cloned.1.call-done) | copy-start | bytes 25165828
  382.5 1.0 copy-start.3
  383.5 118.8 %all-to-all-start.3 = ((bf16[64,6,4096]{2,1,0:T(8,128)(2,1)}), bf16[64,6,4096]{2,1,0:T(8,128)(2,1)}, u32[]{:S(2)}, u32[]{:S(2)}) async-start(bf16[64,6,4096]{2,1,0:T(8,128)(2,1)} %reshape.98), calls=%async_computation.3 | async-start | bytes 8388608 | tf_op jit(solution)/shard_map/all_to_all | solution.py:114
  396.9 90.4 %collective-permute-start = (bf16[15,1024]{1,0:T(8,128)(2,1)S(1)}, bf16[15,1024]{1,0:T(8,128)(2,1)S(1)}, u32[]{:S(2)}, u32[]{:S(2)}) collective-permute-start(bf16[15,1024]{1,0:T(8,128)(2,1)S(1)} %slice.67), channel_id=1, source_target_pairs={{0,4},{4,8},{8,12},{12,16},{16,20},{20,24},{24,28},{28,32},{32,36}... | collective-permute-start | bytes 92168 | tf_op jit(solution)/shard_map/ppermute | solution.py:16
  491.9 2.0 copy-start.1
  498.0 1.6 copy-start.4
  498.1 1.6 copy-start.8
Sparse Core Ops, SparseCore 0:
  135.5 119.3 all-gather.3
  256.7 106.2 all-gather.5
where the time goes:
time: 529 us; the launch traced here: 528 us
  waiting for transfers between devices  287 us (54%)
  blocking collectives  105 us (20%)
  local copies, waits for them, and re-layouts  52.3 us (10%)
  matrix products  25 us (5%)
  other arithmetic  22.6 us (4%)
  starting transfers between devices  20.8 us (4%)
  between operations  14.3 us (3%)
    all_gather x1, waiting for transfers between devices, shards(): piece = lax.all_gather(arrived.reshape(-1, width), 'tp', axis=0, tiled=True)  117 us
    all_to_all x1, blocking collectives, shards(): lax.all_to_all(outgoing, 'ep', split_axis=0, concat_axis=0, tiled=True)  105 us
    ppermute x1, waiting for transfers between devices, from_behind(): return lax.ppermute(x, axis, pairs)  88.1 us
    all_gather x1, waiting for transfers between devices, shards(): piece = lax.all_gather(down_local, 'tp', axis=0, tiled=True)  61.7 us
    all_to_all x1, waiting for transfers between devices, shards(): lax.all_to_all(hidden, 'tp', split_axis=0, concat_axis=1, tiled=True)  20.3 us
  transfers between devices with their start and end apart: 6, of which 4 were waited for; matrix products, arithmetic and copies ran while one was open for 10% of the time, Pallas kernels for 0%

commit v1 on v0

--- a/solution.py
+++ b/solution.py
@@ -100,7 +100,10 @@
     unit_block = lax.all_to_all(hidden, "tp", split_axis=0, concat_axis=1, tiled=True)
     empty = jnp.zeros((unit_block.shape[0], width), jnp.float32)
     total = empty
-    piece = lax.all_gather(down_local, "tp", axis=0, tiled=True)
+    size = lax.axis_size("tp")
+    pieces = jnp.stack([down_local for _ in range(size)])
+    pieces = lax.all_to_all(pieces, "tp", split_axis=0, concat_axis=0)
+    piece = jnp.concatenate(pieces, axis=0)
     for part in range(piece.shape[0] // part_width):
         columns = lax.dynamic_slice_in_dim(unit_block, part * part_width, part_width, 1)
         partial_value = jnp.dot(

time: 529 us -> 544 us (1.028)
  local copies, waits for them, and re-layouts: 52.3 us -> 58.2 us
    all_gather x1, waiting for transfers between devices: 117 us -> 192 us  [shards(): piece = lax.all_gather(arrived.reshape(-1, width), 'tp', axis=0, tiled=True)]
    all_gather x1 -> x0, waiting for transfers between devices: 61.7 us -> none  [shards(): piece = lax.all_gather(down_local, 'tp', axis=0, tiled=True)]
    all_to_all x1, waiting for transfers between devices: 20.3 us -> 11.2 us  [shards(): lax.all_to_all(hidden, 'tp', split_axis=0, concat_axis=1, tiled=True)]
    another operation x3 -> x4, local copies, waits for them, and re-layouts: 1.77 us -> 7.7 us  [the longest x1 5.93 us: shards(): pieces = jnp.stack([down_local for _ in range(size)])]
    all_to_all x0 -> x1, starting transfers between devices: none -> 5.66 us  [shards(): pieces = lax.all_to_all(pieces, 'tp', split_axis=0, concat_axis=0)]
  transfers between devices with their start and end apart: 6 -> 6, of which waited for: 4 -> 3; matrix products, arithmetic and copies ran while one was open for 10% -> 11% of each run, Pallas kernels for 0% -> 0%
where the time goes in v1:
time: 544 us; the launch traced here: 542 us
  waiting for transfers between devices  291 us (53%)
  blocking collectives  105 us (19%)
  local copies, waits for them, and re-layouts  58.2 us (11%)
  matrix products  26.2 us (5%)
  starting transfers between devices  24.3 us (4%)
  other arithmetic  22.6 us (4%)
  between operations  14.3 us (3%)
    all_gather x1, waiting for transfers between devices, shards(): piece = lax.all_gather(arrived.reshape(-1, width), 'tp', axis=0, tiled=True)  192 us
    all_to_all x1, blocking collectives, shards(): lax.all_to_all(outgoing, 'ep', split_axis=0, concat_axis=0, tiled=True)  105 us
    ppermute x1, waiting for transfers between devices, from_behind(): return lax.ppermute(x, axis, pairs)  88.1 us
    all_to_all x1, waiting for transfers between devices, shards(): lax.all_to_all(hidden, 'tp', split_axis=0, concat_axis=1, tiled=True)  11.2 us
  transfers between devices with their start and end apart: 6, of which 3 were waited for; matrix products, arithmetic and copies ran while one was open for 11% of the time, Pallas kernels for 0%

profile of v1, /device:TPU:96, one launch (start us, length us, event | category | flops | bytes accessed | tf_op | source)
XLA Modules:
  0.0 541.9 jit_solution(8709757876134757399)
XLA Ops:
  7.2 0.8 constant_dynamic-slice_fusion.1
  8.5 0.3 multiply_reduce_fusion
  9.0 1.5 fusion.12
  10.6 1.6 fusion.14
  12.1 4.1 gather_fusion
  16.2 5.6 %reshape.107 = bf16[64,6,4096]{2,1,0:T(8,128)(2,1)} reshape(bf16[384,4096]{1,0:T(8,128)(2,1)} %gather_fusion) | data formatting | bytes 6291456 | tf_op jit(solution)/shard_map/gather | solution.py:91
  22.0 2.5 broadcast_multiply_fusion
  24.5 105.1 %all_to_all.53 = bf16[64,6,4096]{2,1,0:T(8,128)(2,1)} all-to-all(bf16[64,6,4096]{2,1,0:T(8,128)(2,1)S(1)} %broadcast_multiply_fusion), channel_id=1, replica_groups=mesh['ep'=64,'tp'=4] {'ep'}, dimensions={0} | all-to-all | bytes 6291456 | tf_op jit(solution)/shard_map/all_to_all | solution.py:92
  129.6 5.7 %reshape.103 = bf16[384,4096]{1,0:T(8,128)(2,1)} reshape(bf16[64,6,4096]{2,1,0:T(8,128)(2,1)} %all_to_all.53) | data formatting | bytes 6291456 | tf_op jit(solution)/shard_map/reshape | solution.py:93
  135.4 5.9 %stack.3 = bf16[4,256,4096]{2,1,0:T(8,128)(2,1)} broadcast(bf16[256,4096]{1,0:T(8,128)(2,1)} %bitcast.62), dimensions={1,2} | broadcast | bytes 10485760 | tf_op jit(solution)/shard_map/stack | solution.py:104
  141.3 5.7 %all-to-all-start.3 = ((bf16[4,256,4096]{2,1,0:T(8,128)(2,1)}), bf16[4,256,4096]{2,1,0:T(8,128)(2,1)}, u32[]{:S(2)}, u32[]{:S(2)}) async-start(bf16[4,256,4096]{2,1,0:T(8,128)(2,1)} %stack.3), calls=%async_computation.3 | async-start | bytes 16777216 | tf_op jit(solution)/shard_map/all_to_all | solution.py:105
  147.0 1.7 copy.27
  148.7 0.6 fusion.9
  149.2 191.8 %all-gather.2.cloned.1.call-done = bf16[1536,4096]{1,0:T(8,128)(2,1)} async-done(((bf16[384,4096]{1,0:T(8,128)(2,1)}), bf16[1536,4096]{1,0:T(8,128)(2,1)}) %all-gather.2.cloned.1.call-update) | async-done | bytes 12582928 | tf_op jit(solution)/shard_map/all_gather | solution.py:93
  341.0 7.7 %convolution_minimum_fusion = f32[1536,256]{1,0:T(8,128)S(1)} fusion(bf16[1536,4096]{1,0:T(8,128)(2,1)} %all-gather.2.cloned.1.call-done, bf16[1,4096,256]{2,1,0:T(8,128)(2,1)} %param.19), kind=kOutput, calls=%fused_computation.10 | convolution fusion | flops 3221618688 | bytes 16252928 | tf_op jit(solution)/shard_map/dot_general | solution.py:95
  348.8 1.0 copy-done.5
  349.8 0.6 copy-done.6
  350.4 4.9 fusion.5
  355.3 2.3 copy.36
  357.6 4.2 all-to-all-start.2
  361.8 1.5 fusion.11
  363.3 11.2 %all-to-all-done.2 = bf16[4,384,256]{1,2,0:T(8,128)(2,1)} async-done(((bf16[4,384,256]{1,2,0:T(8,128)(2,1)}), bf16[4,384,256]{1,2,0:T(8,128)(2,1)}, u32[]{:S(2)}, u32[]{:S(2)}) %all-to-all-start.2) | async-done | bytes 786464 | tf_op jit(solution)/shard_map/all_to_all | solution.py:100
  374.6 3.7 all-to-all-start
  378.3 2.7 convolution_convert_fusion.3
  381.0 2.7 convolution_convert_fusion.2
  383.7 2.7 convolution_convert_fusion.1
  386.5 2.7 convolution_convert_fusion
  389.2 4.1 add_convert_fusion
  393.3 5.6 %reshape.104 = bf16[64,6,4096]{2,1,0:T(8,128)(2,1)} reshape(bf16[384,4096]{1,0:T(8,128)(2,1)} %add_convert_fusion) | data formatting | bytes 6291456 | tf_op jit(solution)/shard_map/reshape | solution.py:116
  399.0 1.0 copy-done.2
  399.9 8.4 %all-to-all-start.4 = ((bf16[64,6,4096]{2,1,0:T(8,128)(2,1)}), bf16[64,6,4096]{2,1,0:T(8,128)(2,1)}, u32[]{:S(2)}, u32[]{:S(2)}) async-start(bf16[64,6,4096]{2,1,0:T(8,128)(2,1)} %reshape.104), calls=%async_computation.4 | async-start | bytes 8388608 | tf_op jit(solution)/shard_map/all_to_all | solution.py:117
  408.4 0.7 constant_dynamic-slice_fusion
  409.1 0.7 multiply_add_fusion
  409.8 1.5 copy.28
  411.3 2.3 collective-permute-start
  413.6 88.1 %collective-permute-done = bf16[15,1024]{1,0:T(8,128)(2,1)S(1)} collective-permute-done((bf16[15,1024]{1,0:T(8,128)(2,1)S(1)}, bf16[15,1024]{1,0:T(8,128)(2,1)S(1)}, u32[]{:S(2)}, u32[]{:S(2)}) %collective-permute-start) | collective-permute-done | bytes 30752 | tf_op jit(solution)/shard_map/ppermute | solution.py:16
  501.7 1.7 fusion.29
  503.3 0.3 pad.4
  503.6 2.6 fusion
  506.2 2.0 copy-done.1
  508.2 2.6 broadcast_add_fusion
  510.9 1.5 copy.30
  512.7 1.3 copy-done.3
  514.0 2.6 multiply_convert_fusion
  516.6 5.7 %reshape.105 = bf16[384,4096]{1,0:T(8,128)(2,1)} reshape(bf16[64,6,4096]{2,1,0:T(8,128)(2,1)} %all-to-all-done.4) | data formatting | bytes 6291456 | tf_op jit(solution)/shard_map/reshape | solution.py:118
  522.4 4.5 gather_fusion.1
  526.9 5.5 %gather_fusion.2 = bf16[128,4096]{1,0:T(8,128)(2,1)} fusion(bf16[384,4096]{1,0:T(8,128)(2,1)} %reshape.105, s32[1024]{0:T(1024)S(1)} %get-tuple-element.10), kind=kCustom, calls=%fused_computation.2 | custom fusion | bytes 2097664 | tf_op jit(solution)/shard_map/gather | solution.py:124
  532.3 2.7 add_convert_fusion.1
  (40 shorter events, 1.2 us)
Async XLA Ops:
  7.2 505.5 %copy-start = (bf16[1,1024,1024]{2,1,0:T(8,128)(2,1)S(1)}, bf16[1,1024,1024]{2,1,0:T(8,128)(2,1)}, u32[]{:S(2)}) copy-start(bf16[1,1024,1024]{2,1,0:T(8,128)(2,1)} %param.13) | copy-start | bytes 6291460
  7.2 333.9 %all-gather.2.cloned.1.call-start = ((), (), s32[]{:S(2)}) async-start(), calls=%async_computation.5 | async-start | bytes 15728640 | tf_op jit(solution)/shard_map/all_gather | solution.py:93
  141.3 216.3 %all-to-all-start.3 = ((bf16[4,256,4096]{2,1,0:T(8,128)(2,1)}), bf16[4,256,4096]{2,1,0:T(8,128)(2,1)}, u32[]{:S(2)}, u32[]{:S(2)}) async-start(bf16[4,256,4096]{2,1,0:T(8,128)(2,1)} %stack.3), calls=%async_computation.3 | async-start | bytes 16777216 | tf_op jit(solution)/shard_map/all_to_all | solution.py:105
  341.0 8.8 %copy-start.5 = (bf16[1536,4096]{1,0:T(8,128)(2,1)S(1)}, bf16[1536,4096]{1,0:T(8,128)(2,1)}, u32[]{:S(2)}) copy-start(bf16[1536,4096]{1,0:T(8,128)(2,1)} %all-gather.2.cloned.1.call-done) | copy-start | bytes 37748740
  341.0 9.4 %copy-start.6 = (bf16[1,4096,256]{2,1,0:T(8,128)(2,1)S(1)}, bf16[1,4096,256]{2,1,0:T(8,128)(2,1)}, u32[]{:S(2)}) copy-start(bf16[1,4096,256]{2,1,0:T(8,128)(2,1)} %param.20) | copy-start | bytes 6291460
  355.3 6.5 %copy-start.4 = (f32[4096]{0:T(1024)S(1)}, f32[4096]{0:T(1024)}, u32[]{:S(2)}) copy-start(f32[4096]{0:T(1024)} %param.12) | copy-start | bytes 49156
  357.6 16.9 %all-to-all-start.2 = ((bf16[4,384,256]{1,2,0:T(8,128)(2,1)}), bf16[4,384,256]{1,2,0:T(8,128)(2,1)}, u32[]{:S(2)}, u32[]{:S(2)}) async-start(bf16[4,384,256]{1,2,0:T(8,128)(2,1)} %copy.36), calls=%async_computation.2 | async-start | bytes 1572864 | tf_op jit(solution)/shard_map/all_to_all | solution.py:100
  374.6 24.4 %all-to-all-start = ((bf16[128,4,1024]{0,2,1:T(8,128)(2,1)}), bf16[128,4,1024]{0,2,1:T(8,128)(2,1)S(1)}, u32[]{:S(2)}, u32[]{:S(2)}) async-start(bf16[128,4,1024]{0,2,1:T(8,128)(2,1)} %bitcast.60), calls=%async_computation | async-start | bytes 2097152 | tf_op jit(solution)/shard_map/all_to_all | solution.py:63
  399.0 1.0 copy-start.2
  399.9 116.7 %all-to-all-start.4 = ((bf16[64,6,4096]{2,1,0:T(8,128)(2,1)}), bf16[64,6,4096]{2,1,0:T(8,128)(2,1)}, u32[]{:S(2)}, u32[]{:S(2)}) async-start(bf16[64,6,4096]{2,1,0:T(8,128)(2,1)} %reshape.104), calls=%async_computation.4 | async-start | bytes 8388608 | tf_op jit(solution)/shard_map/all_to_all | solution.py:117
  411.3 90.4 %collective-permute-start = (bf16[15,1024]{1,0:T(8,128)(2,1)S(1)}, bf16[15,1024]{1,0:T(8,128)(2,1)S(1)}, u32[]{:S(2)}, u32[]{:S(2)}) collective-permute-start(bf16[15,1024]{1,0:T(8,128)(2,1)S(1)} %slice.79), channel_id=1, source_target_pairs={{0,4},{4,8},{8,12},{12,16},{16,20},{20,24},{24,28},{28,32},{32,36}... | collective-permute-start | bytes 92168 | tf_op jit(solution)/shard_map/ppermute | solution.py:16
  506.2 2.0 copy-start.1
  512.4 1.6 copy-start.3
  512.4 1.6 copy-start.7
Sparse Core Ops, SparseCore 0:
  135.5 205.5 all-gather.1
